TPU v7x, 32 devices: a whole 2x2x4 slice. The times are simulated.
32 devices in a mesh: rep: 2 (over y), fs: 4 (over z), tp: 4 (over x, core).
Axes of the slice: x: 2, y: 2, z: 4, core: 2. Of those that a mesh axis runs over, the one named last changes fastest.
Arguments:
- tokens: bfloat16 [8, 192, 2048], P(('rep', 'fs'), None, 'tp'), may hold values from -40 to 40
- ff_first: bfloat16 [2048, 2048], P('fs', 'tp'), may hold values from -0.125 to 0.125
- ff_second: bfloat16 [2048, 2048], P('fs', 'tp'), may hold values from -0.125 to 0.125
- ff_down: bfloat16 [2048, 2048], P('fs', 'tp'), may hold values from -0.125 to 0.125
- mix_stream: bfloat16 [2048, 2048], P('fs', 'tp'), may hold values from -0.125 to 0.125
- mix_gate: bfloat16 [2048, 2048], P('fs', 'tp'), may hold values from -0.125 to 0.125
- mix_down: bfloat16 [2048, 2048], P('fs', 'tp'), may hold values from -0.125 to 0.125
- gain_one: float32 [2048], P('tp'), may hold values from 0.1 to 1.9
- gain_two: float32 [2048], P('tp'), may hold values from 0.1 to 1.9
- gain_three: float32 [2048], P('tp'), may hold values from 0.1 to 1.9
Outputs:
- layer_out: bfloat16 [8, 192, 2048], P(('rep', 'fs'), None, 'tp')
All inputs are finite; a program needn't handle non-finite values.
Results may differ from a plain program's by a relative error of at most 0.01.
Values may be sent and summed in bfloat16 or wider, within the bound.
A program may use at most 64 MiB of HBM per device.

v0:
```python
import jax
import jax.numpy as jnp
from jax import lax
from jax.sharding import PartitionSpec as P

alpha_scale = 2.0**0.5
norm_eps = 1e-05


def product(inputs, weight):
    return jnp.einsum("bsd,df->bsf", inputs, weight, preferred_element_type=jnp.float32)


def widen(local_rows):
    return lax.all_gather(local_rows, "tp", axis=2, tiled=True)


def norm_cols(summed, gain_vec):
    width = summed.shape[-1] * lax.axis_size("tp")
    totals, squares = lax.psum((jnp.sum(summed, axis=-1), jnp.sum(summed * summed, axis=-1)), "tp")
    row_mean = totals / width
    row_var = squares / width - row_mean * row_mean
    normed = (summed - row_mean[..., None]) * lax.rsqrt(row_var[..., None] + norm_eps)
    return (normed * gain_vec[None, None, :]).astype(jnp.bfloat16)


def half_step(local_rows, project_in, project_out, gain_vec):
    whole = widen(local_rows)
    first_act, second_act = project_in(whole)
    hidden = (jax.nn.silu(first_act) * second_act).astype(jnp.bfloat16)
    wide_hidden = lax.all_gather(hidden, "tp", axis=2, tiled=True)
    branch = project_out(wide_hidden)
    return norm_cols(alpha_scale * local_rows.astype(jnp.float32) + 0.5 * branch, gain_vec)


def pool_mix(local_rows, project_in, project_out, gain_vec):
    whole = widen(local_rows)
    stream_act, gate_act = project_in(whole)
    stream = stream_act.astype(jnp.bfloat16)
    length = stream.shape[1]
    channel_group = lax.axis_index("tp") * 4 // lax.axis_size("tp")
    window = lax.shift_left(jnp.int32(2), channel_group)
    later = lax.broadcasted_iota(jnp.int32, (length, length), 0)
    earlier = lax.broadcasted_iota(jnp.int32, (length, length), 1)
    offset = later - earlier
    band = ((offset >= 0) & (offset < window)).astype(jnp.bfloat16)
    window_sums = jnp.einsum("ts,bsc->btc", band, stream, preferred_element_type=jnp.float32)
    counts = jnp.minimum(jnp.arange(length, dtype=jnp.int32) + 1, window).astype(jnp.float32)
    pooled = window_sums / counts[None, :, None] - stream.astype(jnp.float32)
    gated = (pooled * jax.nn.silu(gate_act)).astype(jnp.bfloat16)
    wide_gated = lax.all_gather(gated, "tp", axis=2, tiled=True)
    branch = project_out(wide_gated)
    return norm_cols(alpha_scale * local_rows.astype(jnp.float32) + branch, gain_vec)


def shards(
    tokens,
    ff_first,
    ff_second,
    ff_down,
    mix_stream,
    mix_gate,
    mix_down,
    gain_one,
    gain_two,
    gain_three,
):
    collected = (
        lax.all_gather(ff_first, "fs", axis=0, tiled=True),
        lax.all_gather(ff_second, "fs", axis=0, tiled=True),
        lax.all_gather(ff_down, "fs", axis=0, tiled=True),
        lax.all_gather(mix_stream, "fs", axis=0, tiled=True),
        lax.all_gather(mix_gate, "fs", axis=0, tiled=True),
        lax.all_gather(mix_down, "fs", axis=0, tiled=True),
    )

    def ffn_in(whole):
        return (product(whole, collected[0]), product(whole, collected[1]))

    def ffn_out(wide_rows):
        return product(wide_rows, collected[2])

    def mix_in(whole):
        return (product(whole, collected[3]), product(whole, collected[4]))

    def mix_out(wide_rows):
        return product(wide_rows, collected[5])

    first = half_step(tokens, ffn_in, ffn_out, gain_one)
    second = pool_mix(first, mix_in, mix_out, gain_two)
    return half_step(second, ffn_in, ffn_out, gain_three)


def solution(mesh):
    placed = (
        P(("rep", "fs"), None, "tp"),
        P("fs", "tp"),
        P("fs", "tp"),
        P("fs", "tp"),
        P("fs", "tp"),
        P("fs", "tp"),
        P("fs", "tp"),
        P("tp"),
        P("tp"),
        P("tp"),
    )
    return jax.shard_map(
        shards, mesh=mesh, in_specs=placed, out_specs=P(("rep", "fs"), None, "tp"), check_vma=False
    )
```

profile of v0, /device:TPU:0, one launch (start us, length us, event | category | flops | bytes accessed | tf_op | source)
XLA Modules:
  0.0 329.4 jit_solution(16237052281995979213)
XLA Ops:
  6.5 0.0 all-gather.9.cloned.1.call-start
  6.5 0.7 all-gather.9.cloned.1.call-update
  7.3 0.0 all-gather.11.cloned.1.call-start
  7.3 0.7 all-gather.11.cloned.1.call-update
  8.0 0.0 all-gather.13.cloned.1.call-start
  8.1 0.7 all-gather.13.cloned.1.call-update
  8.7 0.0 all-gather.15.cloned.1.call-start
  8.8 0.5 all-gather.15.cloned.1.call-update
  9.3 0.0 all-gather.17.cloned.1.call-start
  9.4 0.5 all-gather.17.cloned.1.call-update
  9.9 0.0 all-gather.19.cloned.1.call-start
  10.0 0.5 all-gather.19.cloned.1.call-update
  10.5 0.0 copy-done.1
  10.5 10.1 %all_gather.36 = bf16[1,192,2048]{2,1,0:T(8,128)(2,1)S(1)} all-gather(bf16[1,192,512]{2,1,0:T(8,128)(2,1)S(1)} %copy-done.1), channel_id=1, replica_groups=mesh['rep'=2,'fs'=4,'tp'=4] {'tp'}, dimensions={2}, use_global_device_ids=true | all-gather | bytes 983040 | tf_op jit(solution)/shard_map/all_gather | solution.py:15
  20.6 36.7 %all-gather.9.cloned.1.call-done = bf16[2048,512]{1,0:T(8,128)(2,1)} async-done(((bf16[512,512]{1,0:T(8,128)(2,1)}), bf16[2048,512]{1,0:T(8,128)(2,1)}) %all-gather.9.cloned.1.call-update) | async-done | bytes 2097168 | tf_op jit(solution)/shard_map/all_gather | solution.py:69
  57.3 2.2 fusion.20
  59.5 43.9 %all-gather.11.cloned.1.call-done = bf16[2048,512]{1,0:T(8,128)(2,1)} async-done(((bf16[512,512]{1,0:T(8,128)(2,1)}), bf16[2048,512]{1,0:T(8,128)(2,1)}) %all-gather.11.cloned.1.call-update) | async-done | bytes 2097168 | tf_op jit(solution)/shard_map/all_gather | solution.py:70
  103.4 2.2 fusion.5
  105.6 0.0 copy-start.2
  105.6 8.6 %all-gather = bf16[192,2048]{1,0:T(8,128)(2,1)S(1)} all-gather(bf16[192,512]{1,0:T(8,128)(2,1)S(1)} %fusion.5), channel_id=2, replica_groups=mesh['rep'=2,'fs'=4,'tp'=4] {'tp'}, dimensions={1}, use_global_device_ids=true | all-gather | bytes 983040 | tf_op jit(solution)/shard_map/all_gather | solution.py:31
  114.1 35.3 %all-gather.13.cloned.1.call-done = bf16[2048,512]{1,0:T(8,128)(2,1)} async-done(((bf16[512,512]{1,0:T(8,128)(2,1)}), bf16[2048,512]{1,0:T(8,128)(2,1)}) %all-gather.13.cloned.1.call-update) | async-done | bytes 2097168 | tf_op jit(solution)/shard_map/all_gather | solution.py:71
  149.4 2.3 fusion.32
  151.8 6.4 %all-reduce.2 = (f32[1,192]{1,0:T(1,128)S(1)}, f32[1,192]{1,0:T(1,128)S(1)}) all-reduce(f32[1,192]{1,0:T(1,128)S(1)} %bitcast.92, f32[1,192]{1,0:T(1,128)S(1)} %bitcast.91), channel_id=1, replica_groups=mesh['rep'=2,'fs'=4,'tp'=4] {'tp'}, use_global_device_ids=true, to_apply=%region_3.4 | all-reduce | flops 384 | bytes 3072 | tf_op jit(solution)/shard_map/psum | solution.py:20
  158.2 0.0 copy-done.2
  158.2 0.1 multiply_convert_fusion.2
  158.3 8.1 %all_gather.41 = bf16[1,192,2048]{2,1,0:T(8,128)(2,1)S(1)} all-gather(bf16[1,192,512]{2,1,0:T(8,128)(2,1)S(1)} %multiply_convert_fusion.2), channel_id=1, replica_groups=mesh['rep'=2,'fs'=4,'tp'=4] {'tp'}, dimensions={2}, use_global_device_ids=true | all-gather | bytes 983040 | tf_op jit(solution)/shard_map/all_gather | solution.py:15
  166.4 28.9 %all-gather.15.cloned.1.call-done = bf16[2048,512]{1,0:T(8,128)(2,1)} async-done(((bf16[512,512]{1,0:T(8,128)(2,1)}), bf16[2048,512]{1,0:T(8,128)(2,1)}) %all-gather.15.cloned.1.call-update) | async-done | bytes 2097168 | tf_op jit(solution)/shard_map/all_gather | solution.py:72
  195.4 2.2 convolution_convert_fusion
  197.5 43.7 %all-gather.17.cloned.1.call-done = bf16[2048,512]{1,0:T(8,128)(2,1)} async-done(((bf16[512,512]{1,0:T(8,128)(2,1)}), bf16[2048,512]{1,0:T(8,128)(2,1)}) %all-gather.17.cloned.1.call-update) | async-done | bytes 2097168 | tf_op jit(solution)/shard_map/all_gather | solution.py:73
  241.3 2.2 fusion.16
  243.4 0.2 fusion.11
  243.7 0.0 copy-start.3
  243.7 8.6 %all_gather.44 = bf16[1,192,2048]{2,1,0:T(8,128)(2,1)S(1)} all-gather(bf16[1,192,512]{2,1,0:T(8,128)(2,1)S(1)} %fusion.11), channel_id=1, replica_groups=mesh['rep'=2,'fs'=4,'tp'=4] {'tp'}, dimensions={2}, use_global_device_ids=true | all-gather | bytes 983040 | tf_op jit(solution)/shard_map/all_gather | solution.py:51
  252.3 34.9 %all-gather.19.cloned.1.call-done = bf16[2048,512]{1,0:T(8,128)(2,1)} async-done(((bf16[512,512]{1,0:T(8,128)(2,1)}), bf16[2048,512]{1,0:T(8,128)(2,1)}) %all-gather.19.cloned.1.call-update) | async-done | bytes 2097168 | tf_op jit(solution)/shard_map/all_gather | solution.py:74
  287.2 2.3 fusion.31
  289.5 6.4 %all-reduce.1 = (f32[1,192]{1,0:T(1,128)S(1)}, f32[1,192]{1,0:T(1,128)S(1)}) all-reduce(f32[1,192]{1,0:T(1,128)S(1)} %bitcast.88, f32[1,192]{1,0:T(1,128)S(1)} %bitcast.87), channel_id=1, replica_groups=mesh['rep'=2,'fs'=4,'tp'=4] {'tp'}, use_global_device_ids=true, to_apply=%region_7.8 | all-reduce | flops 384 | bytes 3072 | tf_op jit(solution)/shard_map/psum | solution.py:20
  295.9 0.1 multiply_convert_fusion.1
  296.1 8.2 %all_gather.46 = bf16[1,192,2048]{2,1,0:T(8,128)(2,1)S(1)} all-gather(bf16[1,192,512]{2,1,0:T(8,128)(2,1)S(1)} %multiply_convert_fusion.1), channel_id=1, replica_groups=mesh['rep'=2,'fs'=4,'tp'=4] {'tp'}, dimensions={2}, use_global_device_ids=true | all-gather | bytes 983040 | tf_op jit(solution)/shard_map/all_gather | solution.py:15
  304.3 0.6 fusion.13
  304.9 0.0 copy-done.6
  304.9 0.0 copy-start.5
  304.9 0.6 fusion.6
  305.5 0.0 copy-start.4
  305.5 8.8 %all-gather.1 = bf16[192,2048]{1,0:T(8,128)(2,1)S(1)} all-gather(bf16[192,512]{1,0:T(8,128)(2,1)S(1)} %fusion.6), channel_id=3, replica_groups=mesh['rep'=2,'fs'=4,'tp'=4] {'tp'}, dimensions={1}, use_global_device_ids=true | all-gather | bytes 983040 | tf_op jit(solution)/shard_map/all_gather | solution.py:31
  314.4 0.0 copy-done.5
  314.4 0.7 fusion.30
  315.1 6.7 %all-reduce = (f32[1,192]{1,0:T(1,128)S(1)}, f32[1,192]{1,0:T(1,128)S(1)}) all-reduce(f32[1,192]{1,0:T(1,128)S(1)} %bitcast.90, f32[1,192]{1,0:T(1,128)S(1)} %bitcast.89), channel_id=1, replica_groups=mesh['rep'=2,'fs'=4,'tp'=4] {'tp'}, use_global_device_ids=true, to_apply=%region_11.12 | all-reduce | flops 384 | bytes 3072 | tf_op jit(solution)/shard_map/psum | solution.py:20
  321.7 0.8 multiply_convert_fusion
  (10 shorter events, 0.1 us)
Async XLA Ops:
  6.5 4.0 %copy-start.1 = (bf16[1,192,512]{2,1,0:T(8,128)(2,1)S(1)}, bf16[1,192,512]{2,1,0:T(8,128)(2,1)}, u32[]{:S(2)}) copy-start(bf16[1,192,512]{2,1,0:T(8,128)(2,1)} %param.10) | copy-start | bytes 589828
  6.5 50.8 %all-gather.9.cloned.1.call-start = ((), (), s32[]{:S(2)}) async-start(), calls=%async_computation | async-start | bytes 2621440 | tf_op jit(solution)/shard_map/all_gather | solution.py:69
  7.3 96.1 %all-gather.11.cloned.1.call-start = ((), (), s32[]{:S(2)}) async-start(), calls=%async_computation.1 | async-start | bytes 2621440 | tf_op jit(solution)/shard_map/all_gather | solution.py:70
  8.0 141.4 %all-gather.13.cloned.1.call-start = ((), (), s32[]{:S(2)}) async-start(), calls=%async_computation.2 | async-start | bytes 2621440 | tf_op jit(solution)/shard_map/all_gather | solution.py:71
  8.7 186.6 %all-gather.15.cloned.1.call-start = ((), (), s32[]{:S(2)}) async-start(), calls=%async_computation.3 | async-start | bytes 2621440 | tf_op jit(solution)/shard_map/all_gather | solution.py:72
  9.3 232.0 %all-gather.17.cloned.1.call-start = ((), (), s32[]{:S(2)}) async-start(), calls=%async_computation.4 | async-start | bytes 2621440 | tf_op jit(solution)/shard_map/all_gather | solution.py:73
  9.9 277.3 %all-gather.19.cloned.1.call-start = ((), (), s32[]{:S(2)}) async-start(), calls=%async_computation.5 | async-start | bytes 2621440 | tf_op jit(solution)/shard_map/all_gather | solution.py:74
  105.6 52.6 %copy-start.2 = (f32[512]{0:T(512)S(1)}, f32[512]{0:T(512)}, u32[]{:S(2)}) copy-start(f32[512]{0:T(512)} %param.17) | copy-start | bytes 6148
  243.7 52.3 %copy-start.3 = (f32[512]{0:T(512)S(1)}, f32[512]{0:T(512)}, u32[]{:S(2)}) copy-start(f32[512]{0:T(512)} %param.18) | copy-start | bytes 6148
  252.3 52.0 %copy-start = (bf16[2048,512]{1,0:T(8,128)(2,1)S(1)}, bf16[2048,512]{1,0:T(8,128)(2,1)}, u32[]{:S(2)}) copy-start(bf16[2048,512]{1,0:T(8,128)(2,1)} %all-gather.9.cloned.1.call-done) | copy-start | bytes 6291460
  296.1 8.8 %copy-start.6 = (bf16[2048,512]{1,0:T(8,128)(2,1)S(1)}, bf16[2048,512]{1,0:T(8,128)(2,1)}, u32[]{:S(2)}) copy-start(bf16[2048,512]{1,0:T(8,128)(2,1)} %all-gather.11.cloned.1.call-done) | copy-start | bytes 6291460
  304.9 9.4 %copy-start.5 = (bf16[2048,512]{1,0:T(8,128)(2,1)S(1)}, bf16[2048,512]{1,0:T(8,128)(2,1)}, u32[]{:S(2)}) copy-start(bf16[2048,512]{1,0:T(8,128)(2,1)} %all-gather.13.cloned.1.call-done) | copy-start | bytes 6291460
  305.5 16.2 %copy-start.4 = (f32[512]{0:T(512)S(1)}, f32[512]{0:T(512)}, u32[]{:S(2)}) copy-start(f32[512]{0:T(512)} %param.19) | copy-start | bytes 6148
Sparse Core Ops, SparseCore 0:
  8.9 48.3 all-gather.8
  58.9 44.4 all-gather.10
  105.0 44.4 all-gather.12
  150.9 44.4 all-gather.14
  196.8 44.4 all-gather.16
  242.7 44.4 all-gather.18
where the time goes:
time: 330 us; the launch traced here: 329 us
  waiting for transfers between devices  227 us (69%)
  blocking collectives  71.8 us (22%)
  matrix products  15.4 us (5%)
  between operations  13.6 us (4%)
    all_gather x1, waiting for transfers between devices, shards(): lax.all_gather(ff_second, 'fs', axis=0, tiled=True)  43.9 us
    all_gather x1, waiting for transfers between devices, shards(): lax.all_gather(mix_gate, 'fs', axis=0, tiled=True)  43.7 us
    all_gather x1, waiting for transfers between devices, shards(): lax.all_gather(ff_first, 'fs', axis=0, tiled=True)  36.7 us
    all_gather x1, waiting for transfers between devices, shards(): lax.all_gather(ff_down, 'fs', axis=0, tiled=True)  35.3 us
    all_gather x1, waiting for transfers between devices, shards(): lax.all_gather(mix_down, 'fs', axis=0, tiled=True)  34.9 us
    all_gather x1, waiting for transfers between devices, shards(): lax.all_gather(mix_stream, 'fs', axis=0, tiled=True)  28.9 us
    all_gather x3, blocking collectives, widen(): return lax.all_gather(local_rows, 'tp', axis=2, tiled=True)  26.4 us
    psum x3, blocking collectives, norm_cols(): lax.psum((jnp.sum(summed, axis=-1), jnp.sum(summed * summed, axis=-1)), '...  19.4 us
  transfers between devices with their start and end apart: 6, of which 6 were waited for; matrix products, arithmetic and copies ran while one was open for 3% of the time, Pallas kernels for 0%

commit v1 on v0

--- a/solution.py
+++ b/solution.py
@@ -1,6 +1,10 @@
+import functools
+
 import jax
 import jax.numpy as jnp
 from jax import lax
+from jax.experimental import pallas as pl
+from jax.experimental.pallas import tpu as pltpu
 from jax.sharding import PartitionSpec as P
 
 alpha_scale = 2.0**0.5
@@ -91,6 +95,326 @@
     return half_step(second, ffn_in, ffn_out, gain_three)
 
 
+N_WEIGHTS = 6
+MESH = pl.DeviceIdType.MESH
+
+
+def hub_kernel(
+    axis_sizes,
+    tok,
+    wa,
+    wb,
+    wc,
+    ws,
+    wg,
+    wm,
+    gain_one,
+    gain_two,
+    gain_three,
+    out,
+    wbuf,
+    acts,
+    stat,
+    landed,
+    tok_sem,
+    end_send,
+    end_recv,
+    mid_send,
+    mid_recv,
+    rep_send,
+    rep_recv,
+    tp_send,
+    tp_recv,
+    stat_send,
+    stat_recv,
+    out_sem,
+):
+    n_fs, n_tp = axis_sizes
+    weights = (wa, wb, wc, ws, wg, wm)
+    rows, width = tok.shape
+    depth = wa.shape[0]
+    half = depth // 2
+    features = width * n_tp
+    r = lax.axis_index("rep")
+    z = lax.axis_index("fs")
+    j = lax.axis_index("tp")
+    side = r % 2
+    pair = r + 1 - 2 * side
+    core_peer = j + 1 - 2 * (j % 2)
+    chip_peer = (j + 2) % n_tp
+    cross_peer = (core_peer + 2) % n_tp
+    upper = z // 2
+    is_hub = (z + 1) // 2 == 1
+    my_end = upper * (n_fs - 1)
+    my_hub = 1 + upper
+    other_hub = n_fs - 1 - my_hub
+    other_end = n_fs - 1 - my_end
+
+    barrier = pltpu.get_barrier_semaphore()
+
+    def greet(**where):
+        pl.semaphore_signal(barrier, inc=1, device_id=where, device_id_type=MESH)
+
+    greet(tp=core_peer)
+    greet(tp=chip_peer)
+    greet(tp=cross_peer)
+
+    @pl.when(is_hub)
+    def _():
+        greet(rep=pair)
+        greet(fs=other_hub)
+        greet(fs=my_end)
+        pl.semaphore_wait(barrier, 6)
+
+    @pl.when(jnp.logical_not(is_hub))
+    def _():
+        greet(fs=my_hub)
+        pl.semaphore_wait(barrier, 4)
+
+    def remote(src, dst, send_sem, recv_sem, **where):
+        return pltpu.make_async_remote_copy(
+            src_ref=src, dst_ref=dst, send_sem=send_sem, recv_sem=recv_sem, device_id=where, device_id_type=MESH
+        )
+
+    def part(ref, which):
+        return ref.at[pl.ds(pl.multiple_of(which * half, half), half)]
+
+    def seq(ref, s):
+        return ref.at[pl.ds(s * rows, rows)]
+
+    def tok_copy():
+        return remote(tok, seq(acts.at[0, j], 1), tok_sem.at[0], tok_sem.at[1], fs=my_hub)
+
+    def end_copy(w, order):
+        which = side if order == 0 else 1 - side
+        return remote(part(weights[w], which), part(wbuf.at[w, 0], which), end_send.at[w, order], end_recv.at[w, order], fs=my_hub)
+
+    @pl.when(jnp.logical_not(is_hub))
+    def _():
+        started = [tok_copy()] + [end_copy(w, order) for w in range(N_WEIGHTS) for order in range(2)]
+        for copy in started:
+            copy.start()
+        for copy in started:
+            copy.wait_send()
+        remote(landed, landed, out_sem.at[0], out_sem.at[1], fs=my_hub).wait_recv()
+        out[...] = landed[...]
+
+    @pl.when(is_hub)
+    def _():
+        started = []
+
+        def go(copy):
+            copy.start()
+            started.append(copy)
+
+        def own_out(w):
+            go(remote(part(weights[w], side), part(wbuf.at[w, 1], side), mid_send.at[w, 0], mid_recv.at[w, 0], fs=other_hub))
+
+        def end_through(w):
+            end_copy(w, 0).wait_recv()
+            go(remote(part(wbuf.at[w, 0], side), part(wbuf.at[w, 2], side), mid_send.at[w, 1], mid_recv.at[w, 1], fs=other_hub))
+
+        def share(w, slot):
+            piece = part(wbuf.at[w, 1 + slot], side)
+            remote(piece, piece, mid_send.at[w, slot], mid_recv.at[w, slot], fs=other_hub).wait_recv()
+            go(remote(piece, piece, rep_send.at[w, slot], rep_recv.at[w, slot], rep=pair))
+
+        def complete(w):
+            end_copy(w, 1).wait_recv()
+            for slot in range(2):
+                piece = part(wbuf.at[w, 1 + slot], 1 - side)
+                remote(piece, piece, rep_send.at[w, slot], rep_recv.at[w, slot], rep=pair).wait_recv()
+
+        def block_of(k, owner, s):
+            return seq(acts.at[k, owner], s)
+
+        def spread(k, s, src=None):
+            mine = block_of(k, j, s)
+            src = mine if src is None else src
+            go(remote(src, mine, tp_send.at[k, s, 1], tp_recv.at[k, s, 1], tp=chip_peer))
+            go(remote(src, mine, tp_send.at[k, s, 0], tp_recv.at[k, s, 0], tp=core_peer))
+
+        def relay(k, s):
+            there = block_of(k, chip_peer, s)
+            remote(there, there, tp_send.at[k, s, 1], tp_recv.at[k, s, 1], tp=chip_peer).wait_recv()
+            go(remote(there, there, tp_send.at[k, s, 2], tp_recv.at[k, s, 2], tp=core_peer))
+
+        def gathered(k, s):
+            near = block_of(k, core_peer, s)
+            far = block_of(k, cross_peer, s)
+            remote(near, near, tp_send.at[k, s, 0], tp_recv.at[k, s, 0], tp=core_peer).wait_recv()
+            remote(far, far, tp_send.at[k, s, 2], tp_recv.at[k, s, 2], tp=core_peer).wait_recv()
+
+        def product(k, w, picked):
+            at = pl.ds(0, 2 * rows) if picked is None else pl.ds(picked * rows, rows)
+            total = jnp.dot(acts[k, z, at, :], weights[w][...], preferred_element_type=jnp.float32)
+            for slot, owner in ((0, my_end), (1, other_hub), (2, other_end)):
+                total += jnp.dot(acts[k, owner, at, :], wbuf[w, slot], preferred_element_type=jnp.float32)
+            return total
+
+        def stats_out(n, s, summed):
+            lane = lax.broadcasted_iota(jnp.int32, (rows, 128), 1)
+            sums = jnp.sum(summed, axis=1, keepdims=True)
+            squares = jnp.sum(summed * summed, axis=1, keepdims=True)
+            table = jnp.where(lane == 0, sums, jnp.where(lane == 1, squares, 0.0))
+            stat[n, s, j] = table.T[:8]
+            for at, peer in enumerate((chip_peer, cross_peer, core_peer)):
+                go(remote(stat.at[n, s, j], stat.at[n, s, j], stat_send.at[n, s, at], stat_recv.at[n, s, at], tp=peer))
+
+        def normed(n, s, summed, gain_vec):
+            for at, peer in enumerate((chip_peer, cross_peer, core_peer)):
+                remote(stat.at[n, s, peer], stat.at[n, s, peer], stat_send.at[n, s, at], stat_recv.at[n, s, at], tp=peer).wait_recv()
+            table = stat[n, s, 0]
+            for owner in range(1, n_tp):
+                table += stat[n, s, owner]
+            columns = jnp.concatenate([table, jnp.zeros((120, rows), jnp.float32)], axis=0).T
+            row_mean = columns[:, 0:1] / features
+            row_var = columns[:, 1:2] / features - row_mean * row_mean
+            return ((summed - row_mean) * lax.rsqrt(row_var + norm_eps) * gain_vec[...]).astype(jnp.bfloat16)
+
+        def put_act(k, s, value):
+            acts[k, j, pl.ds(s * rows, rows), :] = value
+
+        def get_act(k, s):
+            return acts[k, j, pl.ds(s * rows, rows), :].astype(jnp.float32)
+
+        order = (1, 0)
+        own_out(0)
+        spread(0, 0, tok)
+        own_out(1)
+        put_act(0, 0, tok[...])
+        tok_copy().wait_recv()
+        spread(0, 1)
+        end_through(0)
+        own_out(2)
+        relay(0, 0)
+        share(0, 0)
+        share(1, 0)
+        relay(0, 1)
+        end_through(1)
+        own_out(3)
+        share(0, 1)
+        share(2, 0)
+        for s in order:
+            gathered(0, s)
+        complete(0)
+        first_act = product(0, 0, None)
+        end_through(2)
+        own_out(4)
+        share(1, 1)
+        share(3, 0)
+        complete(1)
+        second_act = product(0, 1, None)
+        hidden = (jax.nn.silu(first_act) * second_act).astype(jnp.bfloat16)
+        for s in order:
+            put_act(1, s, hidden[s * rows : (s + 1) * rows])
+            spread(1, s)
+        end_through(3)
+        own_out(5)
+        share(2, 1)
+        for s in order:
+            relay(1, s)
+        share(4, 0)
+        for s in order:
+            gathered(1, s)
+        complete(2)
+        branch = product(1, 2, None)
+        sums = [None, None]
+        for s in order:
+            sums[s] = alpha_scale * get_act(0, s) + 0.5 * branch[s * rows : (s + 1) * rows]
+            stats_out(0, s, sums[s])
+        end_through(4)
+        share(3, 1)
+        for s in order:
+            put_act(2, s, normed(0, s, sums[s], gain_one))
+            spread(2, s)
+        share(5, 0)
+        for s in order:
+            relay(2, s)
+        for s in order:
+            gathered(2, s)
+        complete(3)
+        stream = product(2, 3, None).astype(jnp.bfloat16)
+        group = j * 4 // n_tp
+        window = 2 * (1 + group % 2) * (1 + 3 * (group // 2))
+        offset = lax.broadcasted_iota(jnp.int32, (rows, rows), 0) - lax.broadcasted_iota(jnp.int32, (rows, rows), 1)
+        band = jnp.where((offset >= 0) & (offset < window), 1.0, 0.0).astype(jnp.bfloat16)
+        counts = jnp.minimum(lax.broadcasted_iota(jnp.int32, (rows, 1), 0) + 1, window).astype(jnp.float32)
+        pooled = [None, None]
+        for s in order:
+            piece = stream[s * rows : (s + 1) * rows]
+            pooled[s] = jnp.dot(band, piece, preferred_element_type=jnp.float32) / counts - piece.astype(jnp.float32)
+        end_through(5)
+        share(4, 1)
+        share(5, 1)
+        complete(4)
+        for s in order:
+            gate_act = product(2, 4, s)
+            put_act(3, s, (pooled[s] * jax.nn.silu(gate_act)).astype(jnp.bfloat16))
+            spread(3, s)
+        complete(5)
+        for s in order:
+            relay(3, s)
+            gathered(3, s)
+            sums[s] = alpha_scale * get_act(2, s) + product(3, 5, s)
+            stats_out(1, s, sums[s])
+            put_act(4, s, normed(1, s, sums[s], gain_two))
+            spread(4, s)
+        for s in order:
+            relay(4, s)
+            gathered(4, s)
+            put_act(5, s, (jax.nn.silu(product(4, 0, s)) * product(4, 1, s)).astype(jnp.bfloat16))
+            spread(5, s)
+        for s in order:
+            relay(5, s)
+            gathered(5, s)
+            sums[s] = alpha_scale * get_act(4, s) + 0.5 * product(5, 2, s)
+            stats_out(2, s, sums[s])
+            result = normed(2, s, sums[s], gain_three)
+            if s == 1:
+                landed[...] = result
+                go(remote(landed, landed, out_sem.at[0], out_sem.at[1], fs=my_end))
+            else:
+                out[...] = result
+        for copy in started:
+            copy.wait_send()
+
+
+def hub_layer(axis_sizes, tokens, *params):
+    batch, rows, width = tokens.shape
+    weights, gains = params[:N_WEIGHTS], params[N_WEIGHTS:]
+    depth, columns = weights[0].shape
+    n_fs, n_tp = axis_sizes
+    whole = pl.BlockSpec(memory_space=pltpu.VMEM)
+    dma = pltpu.SemaphoreType.DMA
+    result = pl.pallas_call(
+        functools.partial(hub_kernel, axis_sizes),
+        out_shape=jax.ShapeDtypeStruct((rows, width), jnp.bfloat16),
+        in_specs=[whole] * (1 + len(params)),
+        out_specs=whole,
+        scratch_shapes=[
+            pltpu.VMEM((N_WEIGHTS, 3, depth, columns), jnp.bfloat16),
+            pltpu.VMEM((6, n_tp, 2 * rows, width), jnp.bfloat16),
+            pltpu.VMEM((3, 2, n_tp, 8, rows), jnp.float32),
+            pltpu.VMEM((rows, width), jnp.bfloat16),
+            dma((2,)),
+            dma((N_WEIGHTS, 2)),
+            dma((N_WEIGHTS, 2)),
+            dma((N_WEIGHTS, 2)),
+            dma((N_WEIGHTS, 2)),
+            dma((N_WEIGHTS, 2)),
+            dma((N_WEIGHTS, 2)),
+            dma((6, 2, 3)),
+            dma((6, 2, 3)),
+            dma((3, 2, 3)),
+            dma((3, 2, 3)),
+            dma((2,)),
+        ],
+        compiler_params=pltpu.CompilerParams(collective_id=0, has_side_effects=True, vmem_limit_bytes=60 * 2**20),
+    )(tokens.reshape(rows, width), *weights, *[gain.reshape(1, -1) for gain in gains])
+    return result.reshape(batch, rows, width)
+
+
 def solution(mesh):
     placed = (
         P(("rep", "fs"), None, "tp"),
@@ -104,6 +428,9 @@
         P("tp"),
         P("tp"),
     )
+    n_rep, n_fs, n_tp = mesh.shape["rep"], mesh.shape["fs"], mesh.shape["tp"]
+    hubs = n_rep % 2 == 0 and n_fs == 4 and n_tp == 4
+    body = functools.partial(hub_layer, (n_fs, n_tp)) if hubs else shards
     return jax.shard_map(
-        shards, mesh=mesh, in_specs=placed, out_specs=P(("rep", "fs"), None, "tp"), check_vma=False
+        body, mesh=mesh, in_specs=placed, out_specs=P(("rep", "fs"), None, "tp"), check_vma=False
     )

time: 330 us -> 129 us (0.39)
  waiting for transfers between devices: 227 us -> 0 us
  Pallas kernels: 0 us -> 127 us
  blocking collectives: 71.8 us -> 0 us
  matrix products: 15.4 us -> 0 us
  between operations: 13.6 us -> 0.01 us
    all_gather x6 -> x0, waiting for transfers between devices: 224 us -> none  [the longest x1 43.9 us: shards(): lax.all_gather(ff_second, 'fs', axis=0, tiled=True)]
    pallas_call x0 -> x1, Pallas kernels: none -> 127 us  [hub_layer(): pl.pallas_call(functools.partial(hub_kernel, axis_sizes), out_shape=jax.S...]
    all_gather x6 -> x0, blocking collectives: 52.4 us -> none  [the longest x3 26.4 us: widen(): return lax.all_gather(local_rows, 'tp', axis=2, tiled=True)]
    psum x3 -> x0, blocking collectives: 19.4 us -> none  [norm_cols(): lax.psum((jnp.sum(summed, axis=-1), jnp.sum(summed * summed, axis=-1)), '...]
    dot_general x10 -> x0, matrix products: 15.4 us -> none  [the longest x9 15.2 us: product(): jnp.einsum('bsd,df->bsf', inputs, weight, preferred_element_type=jnp.floa...]
    unnamed x6 -> x0, waiting for transfers between devices: 3.67 us -> none
  transfers between devices with their start and end apart: 6 -> 0, of which waited for: 6 -> 0; matrix products, arithmetic and copies ran while one was open for 3% -> 0% of each run, Pallas kernels for 0% -> 0%
where the time goes in v1:
time: 129 us
  Pallas kernels  127 us (98%)
  local copies, waits for them, and re-layouts  1.62 us (1%)
    pallas_call x1, Pallas kernels, hub_layer(): pl.pallas_call(functools.partial(hub_kernel, axis_sizes), out_shape=jax.S...  127 us

profile of v1, /device:TPU:0, one launch (start us, length us, event | category | flops | bytes accessed | tf_op | source)
XLA Modules:
  0.0 129.0 jit_solution(6267762691621125495)
XLA Ops:
  0.0 127.4 %shard_map.100 = bf16[192,512]{1,0:T(8,128)(2,1)} custom-call(bf16[192,512]{1,0:T(8,128)(2,1)} %bitcast.6, bf16[512,512]{1,0:T(8,128)(2,1)} %wa.1, bf16[512,512]{1,0:T(8,128)(2,1)} %wb.1, bf16[512,512]{1,0:T(8,128)(2,1)} %wc.1, bf16[512,512]{1,0:T(8,128)(2,1)} %ws.1, bf16[512,512]{1,0:T(8,128)(2,1)} %wg.1, bf16[512,512]{1,0:T(8,128)(2,1)} %wm.1, ...), custom_call_target="tpu_custom_call" | custom-call | tf_op jit(solution)/shard_map/pallas_call | solution.py:390
  127.4 1.6 %copy.12 = bf16[1,192,512]{2,1,0:T(8,128)(2,1)} copy(bf16[1,192,512]{2,1,0:T(8,128)(2,1)} %bitcast.5) | data formatting | bytes 393216

commit v2 on v1

--- a/solution.py
+++ b/solution.py
@@ -191,7 +191,10 @@
 
     @pl.when(jnp.logical_not(is_hub))
     def _():
-        started = [tok_copy()] + [end_copy(w, order) for w in range(N_WEIGHTS) for order in range(2)]
+        started = [tok_copy()] + [end_copy(0, 0)]
+        for w in range(1, N_WEIGHTS):
+            started += [end_copy(w, 0), end_copy(w - 1, 1)]
+        started.append(end_copy(N_WEIGHTS - 1, 1))
         for copy in started:
             copy.start()
         for copy in started:
@@ -279,30 +282,30 @@
             return acts[k, j, pl.ds(s * rows, rows), :].astype(jnp.float32)
 
         order = (1, 0)
+        sums = [None, None]
+        pooled = [None, None]
         own_out(0)
         spread(0, 0, tok)
         own_out(1)
         put_act(0, 0, tok[...])
         tok_copy().wait_recv()
         spread(0, 1)
+        relay(0, 0)
         end_through(0)
+        share(0, 0)
+        end_through(1)
         own_out(2)
-        relay(0, 0)
-        share(0, 0)
         share(1, 0)
         relay(0, 1)
-        end_through(1)
+        share(0, 1)
+        end_through(2)
         own_out(3)
-        share(0, 1)
-        share(2, 0)
+        share(1, 1)
         for s in order:
             gathered(0, s)
         complete(0)
         first_act = product(0, 0, None)
-        end_through(2)
-        own_out(4)
-        share(1, 1)
-        share(3, 0)
+        share(2, 0)
         complete(1)
         second_act = product(0, 1, None)
         hidden = (jax.nn.silu(first_act) * second_act).astype(jnp.bfloat16)
@@ -310,27 +313,29 @@
             put_act(1, s, hidden[s * rows : (s + 1) * rows])
             spread(1, s)
         end_through(3)
-        own_out(5)
+        own_out(4)
         share(2, 1)
-        for s in order:
-            relay(1, s)
-        share(4, 0)
+        relay(1, 1)
+        share(3, 0)
+        relay(1, 0)
         for s in order:
             gathered(1, s)
         complete(2)
         branch = product(1, 2, None)
-        sums = [None, None]
         for s in order:
             sums[s] = alpha_scale * get_act(0, s) + 0.5 * branch[s * rows : (s + 1) * rows]
             stats_out(0, s, sums[s])
         end_through(4)
+        own_out(5)
         share(3, 1)
         for s in order:
             put_act(2, s, normed(0, s, sums[s], gain_one))
             spread(2, s)
-        share(5, 0)
-        for s in order:
-            relay(2, s)
+        share(4, 0)
+        relay(2, 1)
+        relay(2, 0)
+        end_through(5)
+        share(4, 1)
         for s in order:
             gathered(2, s)
         complete(3)
@@ -340,24 +345,24 @@
         offset = lax.broadcasted_iota(jnp.int32, (rows, rows), 0) - lax.broadcasted_iota(jnp.int32, (rows, rows), 1)
         band = jnp.where((offset >= 0) & (offset < window), 1.0, 0.0).astype(jnp.bfloat16)
         counts = jnp.minimum(lax.broadcasted_iota(jnp.int32, (rows, 1), 0) + 1, window).astype(jnp.float32)
-        pooled = [None, None]
         for s in order:
             piece = stream[s * rows : (s + 1) * rows]
             pooled[s] = jnp.dot(band, piece, preferred_element_type=jnp.float32) / counts - piece.astype(jnp.float32)
-        end_through(5)
-        share(4, 1)
-        share(5, 1)
+        share(5, 0)
         complete(4)
         for s in order:
             gate_act = product(2, 4, s)
             put_act(3, s, (pooled[s] * jax.nn.silu(gate_act)).astype(jnp.bfloat16))
             spread(3, s)
+        share(5, 1)
+        for s in order:
+            relay(3, s)
         complete(5)
         for s in order:
-            relay(3, s)
             gathered(3, s)
             sums[s] = alpha_scale * get_act(2, s) + product(3, 5, s)
             stats_out(1, s, sums[s])
+        for s in order:
             put_act(4, s, normed(1, s, sums[s], gain_two))
             spread(4, s)
         for s in order:
@@ -370,12 +375,9 @@
             gathered(5, s)
             sums[s] = alpha_scale * get_act(4, s) + 0.5 * product(5, 2, s)
             stats_out(2, s, sums[s])
-            result = normed(2, s, sums[s], gain_three)
-            if s == 1:
-                landed[...] = result
-                go(remote(landed, landed, out_sem.at[0], out_sem.at[1], fs=my_end))
-            else:
-                out[...] = result
+        landed[...] = normed(2, 1, sums[1], gain_three)
+        go(remote(landed, landed, out_sem.at[0], out_sem.at[1], fs=my_end))
+        out[...] = normed(2, 0, sums[0], gain_three)
         for copy in started:
             copy.wait_send()
 

time: 129 us -> 122 us (0.946)
  Pallas kernels: 127 us -> 120 us
    pallas_call x1, Pallas kernels: 127 us -> 120 us  [hub_layer(): pl.pallas_call(functools.partial(hub_kernel, axis_sizes), out_shape=jax.S...]
where the time goes in v2:
time: 122 us
  Pallas kernels  120 us (98%)
  local copies, waits for them, and re-layouts  1.62 us (1%)
    pallas_call x1, Pallas kernels, hub_layer(): pl.pallas_call(functools.partial(hub_kernel, axis_sizes), out_shape=jax.S...  120 us

profile of v2, /device:TPU:0, one launch (start us, length us, event | category | flops | bytes accessed | tf_op | source)
XLA Modules:
  0.0 121.8 jit_solution(13431810328575843585)
XLA Ops:
  0.0 120.2 %shard_map.100 = bf16[192,512]{1,0:T(8,128)(2,1)} custom-call(bf16[192,512]{1,0:T(8,128)(2,1)} %bitcast.6, bf16[512,512]{1,0:T(8,128)(2,1)} %wa.1, bf16[512,512]{1,0:T(8,128)(2,1)} %wb.1, bf16[512,512]{1,0:T(8,128)(2,1)} %wc.1, bf16[512,512]{1,0:T(8,128)(2,1)} %ws.1, bf16[512,512]{1,0:T(8,128)(2,1)} %wg.1, bf16[512,512]{1,0:T(8,128)(2,1)} %wm.1, ...), custom_call_target="tpu_custom_call" | custom-call | tf_op jit(solution)/shard_map/pallas_call | solution.py:392
  120.2 1.6 %copy.12 = bf16[1,192,512]{2,1,0:T(8,128)(2,1)} copy(bf16[1,192,512]{2,1,0:T(8,128)(2,1)} %bitcast.5) | data formatting | bytes 393216

commit v3 on v2

--- a/solution.py
+++ b/solution.py
@@ -96,6 +96,7 @@
 
 
 N_WEIGHTS = 6
+CUTS = 2
 MESH = pl.DeviceIdType.MESH
 
 
@@ -133,7 +134,8 @@
     weights = (wa, wb, wc, ws, wg, wm)
     rows, width = tok.shape
     depth = wa.shape[0]
-    half = depth // 2
+    half = depth // (2 * CUTS)
+    pieces = N_WEIGHTS * CUTS
     features = width * n_tp
     r = lax.axis_index("rep")
     z = lax.axis_index("fs")
@@ -176,8 +178,8 @@
             src_ref=src, dst_ref=dst, send_sem=send_sem, recv_sem=recv_sem, device_id=where, device_id_type=MESH
         )
 
-    def part(ref, which):
-        return ref.at[pl.ds(pl.multiple_of(which * half, half), half)]
+    def part(ref, u, which):
+        return ref.at[pl.ds(pl.multiple_of((2 * (u % CUTS) + which) * half, half), half)]
 
     def seq(ref, s):
         return ref.at[pl.ds(s * rows, rows)]
@@ -185,16 +187,18 @@
     def tok_copy():
         return remote(tok, seq(acts.at[0, j], 1), tok_sem.at[0], tok_sem.at[1], fs=my_hub)
 
-    def end_copy(w, order):
+    def end_copy(u, order):
         which = side if order == 0 else 1 - side
-        return remote(part(weights[w], which), part(wbuf.at[w, 0], which), end_send.at[w, order], end_recv.at[w, order], fs=my_hub)
+        return remote(part(weights[u // CUTS], u, which), part(wbuf.at[u // CUTS, 0], u, which), end_send.at[u, order], end_recv.at[u, order], fs=my_hub)
 
     @pl.when(jnp.logical_not(is_hub))
     def _():
-        started = [tok_copy()] + [end_copy(0, 0)]
-        for w in range(1, N_WEIGHTS):
-            started += [end_copy(w, 0), end_copy(w - 1, 1)]
-        started.append(end_copy(N_WEIGHTS - 1, 1))
+        ahead = 3
+        started = [tok_copy()] + [end_copy(u, 0) for u in range(ahead)]
+        for u in range(pieces):
+            started.append(end_copy(u, 1))
+            if u + ahead < pieces:
+                started.append(end_copy(u + ahead, 0))
         for copy in started:
             copy.start()
         for copy in started:
@@ -210,23 +214,41 @@
             copy.start()
             started.append(copy)
 
+        def own_piece(u):
+            w = u // CUTS
+            go(remote(part(weights[w], u, side), part(wbuf.at[w, 1], u, side), mid_send.at[u, 0], mid_recv.at[u, 0], fs=other_hub))
+
+        def end_piece(u):
+            w = u // CUTS
+            end_copy(u, 0).wait_recv()
+            go(remote(part(wbuf.at[w, 0], u, side), part(wbuf.at[w, 2], u, side), mid_send.at[u, 1], mid_recv.at[u, 1], fs=other_hub))
+
+        def share_piece(u, slot):
+            piece = part(wbuf.at[u // CUTS, 1 + slot], u, side)
+            remote(piece, piece, mid_send.at[u, slot], mid_recv.at[u, slot], fs=other_hub).wait_recv()
+            go(remote(piece, piece, rep_send.at[u, slot], rep_recv.at[u, slot], rep=pair))
+
+        def of(w):
+            return range(CUTS * w, CUTS * w + CUTS)
+
         def own_out(w):
-            go(remote(part(weights[w], side), part(wbuf.at[w, 1], side), mid_send.at[w, 0], mid_recv.at[w, 0], fs=other_hub))
+            for u in of(w):
+                own_piece(u)
 
         def end_through(w):
-            end_copy(w, 0).wait_recv()
-            go(remote(part(wbuf.at[w, 0], side), part(wbuf.at[w, 2], side), mid_send.at[w, 1], mid_recv.at[w, 1], fs=other_hub))
+            for u in of(w):
+                end_piece(u)
 
         def share(w, slot):
-            piece = part(wbuf.at[w, 1 + slot], side)
-            remote(piece, piece, mid_send.at[w, slot], mid_recv.at[w, slot], fs=other_hub).wait_recv()
-            go(remote(piece, piece, rep_send.at[w, slot], rep_recv.at[w, slot], rep=pair))
+            for u in of(w):
+                share_piece(u, slot)
 
         def complete(w):
-            end_copy(w, 1).wait_recv()
-            for slot in range(2):
-                piece = part(wbuf.at[w, 1 + slot], 1 - side)
-                remote(piece, piece, rep_send.at[w, slot], rep_recv.at[w, slot], rep=pair).wait_recv()
+            for u in of(w):
+                end_copy(u, 1).wait_recv()
+                for slot in range(2):
+                    piece = part(wbuf.at[w, 1 + slot], u, 1 - side)
+                    remote(piece, piece, rep_send.at[u, slot], rep_recv.at[u, slot], rep=pair).wait_recv()
 
         def block_of(k, owner, s):
             return seq(acts.at[k, owner], s)
@@ -290,12 +312,14 @@
         put_act(0, 0, tok[...])
         tok_copy().wait_recv()
         spread(0, 1)
+        for u in of(0):
+            end_piece(u)
+            share_piece(u, 0)
         relay(0, 0)
-        end_through(0)
-        share(0, 0)
-        end_through(1)
+        for u in of(1):
+            end_piece(u)
+            share_piece(u, 0)
         own_out(2)
-        share(1, 0)
         relay(0, 1)
         share(0, 1)
         end_through(2)
@@ -400,12 +424,12 @@
             pltpu.VMEM((3, 2, n_tp, 8, rows), jnp.float32),
             pltpu.VMEM((rows, width), jnp.bfloat16),
             dma((2,)),
-            dma((N_WEIGHTS, 2)),
-            dma((N_WEIGHTS, 2)),
-            dma((N_WEIGHTS, 2)),
-            dma((N_WEIGHTS, 2)),
-            dma((N_WEIGHTS, 2)),
-            dma((N_WEIGHTS, 2)),
+            dma((N_WEIGHTS * CUTS, 2)),
+            dma((N_WEIGHTS * CUTS, 2)),
+            dma((N_WEIGHTS * CUTS, 2)),
+            dma((N_WEIGHTS * CUTS, 2)),
+            dma((N_WEIGHTS * CUTS, 2)),
+            dma((N_WEIGHTS * CUTS, 2)),
             dma((6, 2, 3)),
             dma((6, 2, 3)),
             dma((3, 2, 3)),

time: 122 us -> 125 us (1.025)
  Pallas kernels: 120 us -> 124 us
    pallas_call x1, Pallas kernels: 120 us -> 124 us  [hub_layer(): pl.pallas_call(functools.partial(hub_kernel, axis_sizes), out_shape=jax.S...]
where the time goes in v3:
time: 125 us
  Pallas kernels  124 us (99%)
  local copies, waits for them, and re-layouts  1.62 us (1%)
    pallas_call x1, Pallas kernels, hub_layer(): pl.pallas_call(functools.partial(hub_kernel, axis_sizes), out_shape=jax.S...  124 us

profile of v3, /device:TPU:0, one launch (start us, length us, event | category | flops | bytes accessed | tf_op | source)
XLA Modules:
  0.0 125.2 jit_solution(13440217973688430565)
XLA Ops:
  0.0 123.6 %shard_map.100 = bf16[192,512]{1,0:T(8,128)(2,1)} custom-call(bf16[192,512]{1,0:T(8,128)(2,1)} %bitcast.6, bf16[512,512]{1,0:T(8,128)(2,1)} %wa.1, bf16[512,512]{1,0:T(8,128)(2,1)} %wb.1, bf16[512,512]{1,0:T(8,128)(2,1)} %wc.1, bf16[512,512]{1,0:T(8,128)(2,1)} %ws.1, bf16[512,512]{1,0:T(8,128)(2,1)} %wg.1, bf16[512,512]{1,0:T(8,128)(2,1)} %wm.1, ...), custom_call_target="tpu_custom_call" | custom-call | tf_op jit(solution)/shard_map/pallas_call | solution.py:416
  123.6 1.6 %copy.12 = bf16[1,192,512]{2,1,0:T(8,128)(2,1)} copy(bf16[1,192,512]{2,1,0:T(8,128)(2,1)} %bitcast.5) | data formatting | bytes 393216

commit v4 on v2

--- a/solution.py
+++ b/solution.py
@@ -222,11 +222,17 @@
             remote(piece, piece, mid_send.at[w, slot], mid_recv.at[w, slot], fs=other_hub).wait_recv()
             go(remote(piece, piece, rep_send.at[w, slot], rep_recv.at[w, slot], rep=pair))
 
+        def shared(w, slot):
+            piece = part(wbuf.at[w, 1 + slot], 1 - side)
+            remote(piece, piece, rep_send.at[w, slot], rep_recv.at[w, slot], rep=pair).wait_recv()
+
+        def mostly(w):
+            end_copy(w, 1).wait_recv()
+            shared(w, 0)
+
         def complete(w):
-            end_copy(w, 1).wait_recv()
-            for slot in range(2):
-                piece = part(wbuf.at[w, 1 + slot], 1 - side)
-                remote(piece, piece, rep_send.at[w, slot], rep_recv.at[w, slot], rep=pair).wait_recv()
+            mostly(w)
+            shared(w, 1)
 
         def block_of(k, owner, s):
             return seq(acts.at[k, owner], s)
@@ -248,12 +254,19 @@
             remote(near, near, tp_send.at[k, s, 0], tp_recv.at[k, s, 0], tp=core_peer).wait_recv()
             remote(far, far, tp_send.at[k, s, 2], tp_recv.at[k, s, 2], tp=core_peer).wait_recv()
 
-        def product(k, w, picked):
+        def early(k, w, picked):
             at = pl.ds(0, 2 * rows) if picked is None else pl.ds(picked * rows, rows)
             total = jnp.dot(acts[k, z, at, :], weights[w][...], preferred_element_type=jnp.float32)
-            for slot, owner in ((0, my_end), (1, other_hub), (2, other_end)):
+            for slot, owner in ((0, my_end), (1, other_hub)):
                 total += jnp.dot(acts[k, owner, at, :], wbuf[w, slot], preferred_element_type=jnp.float32)
             return total
+
+        def late(k, w, picked):
+            at = pl.ds(0, 2 * rows) if picked is None else pl.ds(picked * rows, rows)
+            return jnp.dot(acts[k, other_end, at, :], wbuf[w, 2], preferred_element_type=jnp.float32)
+
+        def product(k, w, picked):
+            return early(k, w, picked) + late(k, w, picked)
 
         def stats_out(n, s, summed):
             lane = lax.broadcasted_iota(jnp.int32, (rows, 128), 1)
@@ -349,18 +362,23 @@
             piece = stream[s * rows : (s + 1) * rows]
             pooled[s] = jnp.dot(band, piece, preferred_element_type=jnp.float32) / counts - piece.astype(jnp.float32)
         share(5, 0)
-        complete(4)
-        for s in order:
-            gate_act = product(2, 4, s)
+        mostly(4)
+        gate_early = early(2, 4, None)
+        shared(4, 1)
+        for s in order:
+            gate_act = gate_early[s * rows : (s + 1) * rows] + late(2, 4, s)
             put_act(3, s, (pooled[s] * jax.nn.silu(gate_act)).astype(jnp.bfloat16))
             spread(3, s)
         share(5, 1)
-        for s in order:
-            relay(3, s)
-        complete(5)
+        relay(3, 1)
+        mostly(5)
         for s in order:
             gathered(3, s)
-            sums[s] = alpha_scale * get_act(2, s) + product(3, 5, s)
+            sums[s] = alpha_scale * get_act(2, s) + early(3, 5, s)
+            if s == order[0]:
+                relay(3, 0)
+                shared(5, 1)
+            sums[s] += late(3, 5, s)
             stats_out(1, s, sums[s])
         for s in order:
             put_act(4, s, normed(1, s, sums[s], gain_two))

time: 122 us -> 122 us (level)
  no operation moved by 1% of the time
where the time goes in v4:
time: 122 us; the launch traced here: 121 us
  Pallas kernels  120 us (98%)
  local copies, waits for them, and re-layouts  1.62 us (1%)
    pallas_call x1, Pallas kernels, hub_layer(): pl.pallas_call(functools.partial(hub_kernel, axis_sizes), out_shape=jax.S...  120 us

profile of v4, /device:TPU:0, one launch (start us, length us, event | category | flops | bytes accessed | tf_op | source)
XLA Modules:
  0.0 121.5 jit_solution(12410950900403907492)
XLA Ops:
  0.0 119.9 %shard_map.100 = bf16[192,512]{1,0:T(8,128)(2,1)} custom-call(bf16[192,512]{1,0:T(8,128)(2,1)} %bitcast.6, bf16[512,512]{1,0:T(8,128)(2,1)} %wa.1, bf16[512,512]{1,0:T(8,128)(2,1)} %wb.1, bf16[512,512]{1,0:T(8,128)(2,1)} %wc.1, bf16[512,512]{1,0:T(8,128)(2,1)} %ws.1, bf16[512,512]{1,0:T(8,128)(2,1)} %wg.1, bf16[512,512]{1,0:T(8,128)(2,1)} %wm.1, ...), custom_call_target="tpu_custom_call" | custom-call | tf_op jit(solution)/shard_map/pallas_call | solution.py:410
  119.9 1.6 %copy.12 = bf16[1,192,512]{2,1,0:T(8,128)(2,1)} copy(bf16[1,192,512]{2,1,0:T(8,128)(2,1)} %bitcast.5) | data formatting | bytes 393216
